TPU v7x, 512 devices: a whole 4x4x16 slice. The times are simulated.
512 devices in a mesh: sp: 32 (over z, core), tp: 16 (over y, x).
Axes of the slice: x: 4, y: 4, z: 16, core: 2. Of those that a mesh axis runs over, the one named last changes fastest.
Arguments:
- stream: bfloat16 [12288, 2048], P('sp', 'tp'), may hold values from -6 to 6
- doc_ids: int32 [12288], P('sp'), may hold values from 0 to 9, never falling along the last dimension, each value on 1 to 2304 neighbouring positions
- w_value: bfloat16 [3, 2048, 2048], P(None, None, 'tp'), may hold values from -0.125 to 0.125
- w_gate: bfloat16 [3, 2048, 2048], P(None, None, 'tp'), may hold values from -0.125 to 0.125
- conv_kernel: bfloat16 [3, 31, 2048], P(None, None, 'tp'), may hold values from -4 to 4
- conv_gain: float32 [3, 2048], replicated, may hold values from 0.1 to 1.9
- conv_shift: float32 [3, 2048], replicated, may hold values from -3 to 3
- w_proj: bfloat16 [3, 2048, 2048], P(None, None, 'tp'), may hold values from -0.125 to 0.125
- out_gain: float32 [3, 2048], replicated, may hold values from 0.1 to 1.9
- out_shift: float32 [3, 2048], replicated, may hold values from -3 to 3
Outputs:
- result: bfloat16 [12288, 2048], P('sp', 'tp')
All inputs are finite; a program needn't handle non-finite values.
Results may differ from a plain program's by a relative error of at most 0.013.
Values may be sent and summed in bfloat16 or wider, within the bound.
A program may use at most 64 MiB of HBM per device.

v0:
```python
import jax
import jax.numpy as jnp
from jax import lax
from jax.sharding import Mesh
from jax.sharding import PartitionSpec as P

KERNEL = 31
LAYERS = 3
HALF = 15
TP = ("tp_0", "tp_1")


ALPHA = 2.0**0.25
EPS = 1e-05


def laid_out(tiles, dim):
    tiles = jnp.moveaxis(tiles, 0, dim)
    lengths = tiles.shape
    return tiles.reshape(*lengths[:dim], lengths[dim] * lengths[dim + 1], *lengths[dim + 2 :])


def from_everyone(array, axis):
    devices = lax.axis_size(axis)
    return lax.all_to_all(
        jnp.broadcast_to(array[None], (devices, *array.shape)), axis, 0, 0, tiled=True
    )


def gather_directly(array, axis, dim):
    return laid_out(from_everyone(array, axis), dim)


def padded(block, sides, width):
    for axis, dim in sides:
        count = lax.axis_size(axis)
        forward = [(i, i + 1) for i in range(count - 1)]
        backward = [(target, source) for source, target in forward]
        low = lax.ppermute(
            lax.slice_in_dim(block, block.shape[dim] - width, None, axis=dim), axis, forward
        )
        high = lax.ppermute(lax.slice_in_dim(block, 0, width, axis=dim), axis, backward)
        block = jnp.concatenate([low, block, high], axis=dim)
    return block


def by_axis(array, axes):
    for axis in axes:
        array = lax.psum(array, axis)
    return array


def add_product(piece, weight):
    return jnp.dot(piece, weight, preferred_element_type=jnp.float32)


def on_device(
    stream,
    doc_ids,
    w_value,
    w_gate,
    conv_kernel,
    conv_gain,
    conv_shift,
    w_proj,
    out_gain,
    out_shift,
):
    rows = stream.shape[0]
    local_d = stream.shape[1]
    local_c = w_value.shape[2]
    width_d = w_value.shape[1]
    tp_index = lax.axis_index(TP)
    first_row = lax.axis_index("sp") * rows
    total_rows = rows * lax.axis_size("sp")
    col_d = tp_index * local_d
    hidden, seg_wide = (stream, doc_ids)
    for layer in range(LAYERS):
        value_w = w_value[layer]
        gate_w = w_gate[layer]
        piece = gather_directly(hidden, TP, 1)
        lin = add_product(piece, value_w)
        gat = add_product(piece, gate_w)
        glu = (lin * jax.nn.sigmoid(gat)).astype(jnp.bfloat16)
        glu_wide, seg_here = (padded(glu, (("sp", 0),), HALF), padded(doc_ids, (("sp", 0),), HALF))
        start_pos = first_row - HALF
        residual = hidden
        out_rows = glu_wide.shape[0] - 2 * HALF
        positions = start_pos + jnp.arange(glu_wide.shape[0], dtype=jnp.int32)
        inside = (positions >= 0) & (positions < total_rows)
        centre_seg = seg_here[HALF : HALF + out_rows]
        taps = conv_kernel[layer].astype(jnp.float32)
        glu_float = glu_wide.astype(jnp.float32)
        total = jnp.zeros((out_rows, local_c), jnp.float32)
        for k in range(KERNEL):
            keep = ((seg_here[k : k + out_rows] == centre_seg) & inside[k : k + out_rows]).astype(
                jnp.float32
            )[:, None]
            total = total + glu_float[k : k + out_rows] * keep * taps[k][None, :]
        conv = total.astype(jnp.bfloat16)
        gathered = gather_directly(conv, TP, 1).astype(jnp.float32)
        centre = jnp.mean(gathered, axis=1, keepdims=True)
        spread = jnp.mean(jnp.square(gathered - centre), axis=1, keepdims=True)
        act = jax.nn.silu(
            (gathered - centre) * lax.rsqrt(spread + EPS) * conv_gain[layer] + conv_shift[layer]
        ).astype(jnp.bfloat16)
        branch_out = jnp.dot(act, w_proj[layer], preferred_element_type=jnp.float32)
        mixed = ALPHA * residual.astype(jnp.float32) + branch_out
        tot_one, tot_two = (
            by_axis(jnp.sum(mixed, axis=1), TP),
            by_axis(jnp.sum(mixed * mixed, axis=1), TP),
        )
        mean_z = (tot_one / width_d)[:, None]
        var_z = (tot_two / width_d)[:, None] - mean_z * mean_z
        gain_out = lax.dynamic_slice_in_dim(out_gain[layer], col_d, local_d, 0)
        shift_out = lax.dynamic_slice_in_dim(out_shift[layer], col_d, local_d, 0)
        hidden = ((mixed - mean_z) * lax.rsqrt(var_z + EPS) * gain_out + shift_out).astype(
            jnp.bfloat16
        )
    return hidden


def solution(mesh):
    split = Mesh(mesh.devices.reshape(mesh.shape["sp"], 4, 4), ("sp", "tp_0", "tp_1"))
    return jax.shard_map(
        on_device,
        mesh=split,
        in_specs=(
            P("sp", TP),
            P("sp"),
            P(None, None, TP),
            P(None, None, TP),
            P(None, None, TP),
            P(),
            P(),
            P(None, None, TP),
            P(),
            P(),
        ),
        out_specs=P("sp", TP),
        check_vma=False,
    )
```

profile of v0, /device:TPU:98, one launch (start us, length us, event | category | flops | bytes accessed | tf_op | source)
XLA Modules:
  0.0 279.3 jit_solution(10133785718884650807)
XLA Ops:
  0.0 1.0 copy.15
  1.0 1.4 broadcast_in_dim.12
  2.4 7.6 %all-to-all-start = ((bf16[16,384,128]{1,2,0:T(8,128)(2,1)}), bf16[16,384,128]{1,2,0:T(8,128)(2,1)S(1)}, u32[]{:S(2)}, u32[]{:S(2)}) async-start(bf16[16,384,128]{1,2,0:T(8,128)(2,1)} %broadcast_in_dim.12), calls=%async_computation | async-start | bytes 3145728 | tf_op jit(solution)/shard_map/all_to_all | solution.py:25
  10.1 1.9 collective-permute-start.3
  12.0 2.4 collective-permute-start.2
  14.6 2.3 collective-permute-done.2
  17.2 14.3 %all-to-all-done = bf16[16,384,128]{1,2,0:T(8,128)(2,1)S(1)} async-done(((bf16[16,384,128]{1,2,0:T(8,128)(2,1)}), bf16[16,384,128]{1,2,0:T(8,128)(2,1)S(1)}, u32[]{:S(2)}, u32[]{:S(2)}) %all-to-all-start) | async-done | bytes 1572896 | tf_op jit(solution)/shard_map/all_to_all | solution.py:25
  31.5 1.7 fusion.61
  33.2 1.7 fusion.48
  34.9 1.9 collective-permute-start
  36.8 3.6 %collective-permute-start.1 = (bf16[15,128]{1,0:T(8,128)(2,1)S(1)}, bf16[15,128]{1,0:T(8,128)(2,1)S(1)}, u32[]{:S(2)}, u32[]{:S(2)}) collective-permute-start(bf16[15,128]{1,0:T(8,128)(2,1)S(1)} %get-tuple-element.28), channel_id=1, source_target_pairs={{16,0},{32,16},{48,32},{64,48},{80,64},{96,80},{112,96},{128,112},... | collective-permute-start | bytes 11528 | tf_op jit(solution)/shard_map/ppermute | solution.py:42
  40.5 2.0 collective-permute-done.1
  42.6 2.1 fusion.198
  44.8 0.1 copy.17
  44.9 1.4 broadcast_in_dim.13
  46.3 6.7 %all-to-all-start.1 = ((bf16[16,384,128]{1,2,0:T(8,128)(2,1)}), bf16[16,384,128]{1,2,0:T(8,128)(2,1)S(1)}, u32[]{:S(2)}, u32[]{:S(2)}) async-start(bf16[16,384,128]{1,2,0:T(8,128)(2,1)} %broadcast_in_dim.13), calls=%async_computation.1 | async-start | bytes 3145728 | tf_op jit(solution)/shard_map/all_to_all | solution.py:25
  53.1 20.4 %all-to-all-done.1 = bf16[16,384,128]{1,2,0:T(8,128)(2,1)S(1)} async-done(((bf16[16,384,128]{1,2,0:T(8,128)(2,1)}), bf16[16,384,128]{1,2,0:T(8,128)(2,1)S(1)}, u32[]{:S(2)}, u32[]{:S(2)}) %all-to-all-start.1) | async-done | bytes 1572896 | tf_op jit(solution)/shard_map/all_to_all | solution.py:25
  73.6 0.3 convert_reduce_fusion.2
  73.9 0.5 fusion.26
  74.4 1.3 fusion.35
  75.7 1.5 fusion.329
  77.2 9.0 %all-reduce.5 = (f32[384]{0:T(512)S(1)}, f32[384]{0:T(512)S(1)}) all-reduce(f32[384]{0:T(512)S(1)} %get-tuple-element.10, f32[384]{0:T(512)S(1)} %get-tuple-element.9), channel_id=1, replica_groups=mesh['sp'=32,'tp_0'=4,'tp_1'=4] {'tp_0'}, use_global_device_ids=true, to_apply=%region_6.7 | all-reduce | flops 768 | bytes 6144 | tf_op jit(solution)/shard_map/psum | solution.py:49
  86.3 9.4 %all-reduce.2 = (f32[384]{0:T(512)S(1)}, f32[384]{0:T(512)S(1)}) all-reduce(f32[384]{0:T(512)S(1)} %get-tuple-element.21, f32[384]{0:T(512)S(1)} %get-tuple-element.22), channel_id=1, replica_groups=mesh['sp'=32,'tp_0'=4,'tp_1'=4] {'tp_1'}, use_global_device_ids=true, to_apply=%region_7.8 | all-reduce | flops 768 | bytes 6144 | tf_op jit(solution)/shard_map/psum | solution.py:49
  95.7 0.1 add_convert_fusion.2
  95.8 1.4 broadcast_in_dim.14
  97.2 4.1 %all-to-all-start.2 = ((bf16[16,384,128]{1,2,0:T(8,128)(2,1)}), bf16[16,384,128]{1,2,0:T(8,128)(2,1)S(1)}, u32[]{:S(2)}, u32[]{:S(2)}) async-start(bf16[16,384,128]{1,2,0:T(8,128)(2,1)} %broadcast_in_dim.14), calls=%async_computation.2 | async-start | bytes 3145728 | tf_op jit(solution)/shard_map/all_to_all | solution.py:25
  101.2 20.5 %all-to-all-done.2 = bf16[16,384,128]{1,2,0:T(8,128)(2,1)S(1)} async-done(((bf16[16,384,128]{1,2,0:T(8,128)(2,1)}), bf16[16,384,128]{1,2,0:T(8,128)(2,1)S(1)}, u32[]{:S(2)}, u32[]{:S(2)}) %all-to-all-start.2) | async-done | bytes 1572896 | tf_op jit(solution)/shard_map/all_to_all | solution.py:25
  121.7 0.6 fusion.57
  122.4 1.7 fusion.49
  124.1 1.9 collective-permute-start.4
  126.0 3.6 %collective-permute-start.5 = (bf16[15,128]{1,0:T(8,128)(2,1)S(1)}, bf16[15,128]{1,0:T(8,128)(2,1)S(1)}, u32[]{:S(2)}, u32[]{:S(2)}) collective-permute-start(bf16[15,128]{1,0:T(8,128)(2,1)S(1)} %get-tuple-element.26), channel_id=1, source_target_pairs={{16,0},{32,16},{48,32},{64,48},{80,64},{96,80},{112,96},{128,112},... | collective-permute-start | bytes 11528 | tf_op jit(solution)/shard_map/ppermute | solution.py:42
  129.7 6.9 %collective-permute-done.5 = bf16[15,128]{1,0:T(8,128)(2,1)S(1)} collective-permute-done((bf16[15,128]{1,0:T(8,128)(2,1)S(1)}, bf16[15,128]{1,0:T(8,128)(2,1)S(1)}, u32[]{:S(2)}, u32[]{:S(2)}) %collective-permute-start.5) | collective-permute-done | bytes 3872 | tf_op jit(solution)/shard_map/ppermute | solution.py:42
  136.6 2.1 fusion.136
  138.7 0.1 copy.18
  138.8 0.2 broadcast_in_dim.15
  139.1 24.9 %all_to_all.30 = bf16[16,384,128]{1,2,0:T(8,128)(2,1)S(1)} all-to-all(bf16[16,384,128]{1,2,0:T(8,128)(2,1)S(1)} %broadcast_in_dim.15), channel_id=1, replica_groups=mesh['sp'=32,'tp_0'=4,'tp_1'=4] {'tp_0','tp_1'}, dimensions={0} | all-to-all | bytes 3145728 | tf_op jit(solution)/shard_map/all_to_all | solution.py:25
  163.9 0.3 convert_reduce_fusion.1
  164.3 0.5 fusion.16
  164.8 1.3 fusion.25
  166.1 1.6 fusion.328
  167.6 8.9 %all-reduce.4 = (f32[384]{0:T(512)S(1)}, f32[384]{0:T(512)S(1)}) all-reduce(f32[384]{0:T(512)S(1)} %get-tuple-element.8, f32[384]{0:T(512)S(1)} %get-tuple-element.7), channel_id=1, replica_groups=mesh['sp'=32,'tp_0'=4,'tp_1'=4] {'tp_0'}, use_global_device_ids=true, to_apply=%region_14.15 | all-reduce | flops 768 | bytes 6144 | tf_op jit(solution)/shard_map/psum | solution.py:49
  176.5 9.1 %all-reduce.1 = (f32[384]{0:T(512)S(1)}, f32[384]{0:T(512)S(1)}) all-reduce(f32[384]{0:T(512)S(1)} %get-tuple-element.19, f32[384]{0:T(512)S(1)} %get-tuple-element.20), channel_id=1, replica_groups=mesh['sp'=32,'tp_0'=4,'tp_1'=4] {'tp_1'}, use_global_device_ids=true, to_apply=%region_15.16 | all-reduce | flops 768 | bytes 6144 | tf_op jit(solution)/shard_map/psum | solution.py:49
  185.6 0.1 add_convert_fusion.1
  185.7 1.4 broadcast_in_dim.16
  187.1 4.1 %all-to-all-start.4 = ((bf16[16,384,128]{1,2,0:T(8,128)(2,1)}), bf16[16,384,128]{1,2,0:T(8,128)(2,1)S(1)}, u32[]{:S(2)}, u32[]{:S(2)}) async-start(bf16[16,384,128]{1,2,0:T(8,128)(2,1)} %broadcast_in_dim.16), calls=%async_computation.4 | async-start | bytes 3145728 | tf_op jit(solution)/shard_map/all_to_all | solution.py:25
  191.2 20.0 %all-to-all-done.4 = bf16[16,384,128]{1,2,0:T(8,128)(2,1)S(1)} async-done(((bf16[16,384,128]{1,2,0:T(8,128)(2,1)}), bf16[16,384,128]{1,2,0:T(8,128)(2,1)S(1)}, u32[]{:S(2)}, u32[]{:S(2)}) %all-to-all-start.4) | async-done | bytes 1572896 | tf_op jit(solution)/shard_map/all_to_all | solution.py:25
  211.2 0.6 fusion.53
  211.9 1.7 fusion.50
  213.6 1.9 collective-permute-start.6
  215.5 3.6 %collective-permute-start.7 = (bf16[15,128]{1,0:T(8,128)(2,1)S(1)}, bf16[15,128]{1,0:T(8,128)(2,1)S(1)}, u32[]{:S(2)}, u32[]{:S(2)}) collective-permute-start(bf16[15,128]{1,0:T(8,128)(2,1)S(1)} %get-tuple-element.24), channel_id=1, source_target_pairs={{16,0},{32,16},{48,32},{64,48},{80,64},{96,80},{112,96},{128,112},... | collective-permute-start | bytes 11528 | tf_op jit(solution)/shard_map/ppermute | solution.py:42
  219.2 1.3 collective-permute-done.7
  220.5 2.1 fusion.74
  222.6 0.1 copy.19
  222.7 1.4 broadcast_in_dim.17
  224.1 5.7 %all-to-all-start.5 = ((bf16[16,384,128]{1,2,0:T(8,128)(2,1)}), bf16[16,384,128]{1,2,0:T(8,128)(2,1)S(1)}, u32[]{:S(2)}, u32[]{:S(2)}) async-start(bf16[16,384,128]{1,2,0:T(8,128)(2,1)} %broadcast_in_dim.17), calls=%async_computation.5 | async-start | bytes 3145728 | tf_op jit(solution)/shard_map/all_to_all | solution.py:25
  229.8 24.1 %all-to-all-done.5 = bf16[16,384,128]{1,2,0:T(8,128)(2,1)S(1)} async-done(((bf16[16,384,128]{1,2,0:T(8,128)(2,1)}), bf16[16,384,128]{1,2,0:T(8,128)(2,1)S(1)}, u32[]{:S(2)}, u32[]{:S(2)}) %all-to-all-start.5) | async-done | bytes 1572896 | tf_op jit(solution)/shard_map/all_to_all | solution.py:25
  253.9 0.3 convert_reduce_fusion
  254.2 0.5 fusion.6
  254.7 1.3 fusion.15
  256.0 1.5 fusion.327
  257.5 10.7 %all-reduce.3 = (f32[384]{0:T(512)S(1)}, f32[384]{0:T(512)S(1)}) all-reduce(f32[384]{0:T(512)S(1)} %get-tuple-element.6, f32[384]{0:T(512)S(1)} %get-tuple-element.5), channel_id=1, replica_groups=mesh['sp'=32,'tp_0'=4,'tp_1'=4] {'tp_0'}, use_global_device_ids=true, to_apply=%region_22.23 | all-reduce | flops 768 | bytes 6144 | tf_op jit(solution)/shard_map/psum | solution.py:49
  268.2 10.2 %all-reduce = (f32[384]{0:T(512)S(1)}, f32[384]{0:T(512)S(1)}) all-reduce(f32[384]{0:T(512)S(1)} %get-tuple-element.17, f32[384]{0:T(512)S(1)} %get-tuple-element.18), channel_id=1, replica_groups=mesh['sp'=32,'tp_0'=4,'tp_1'=4] {'tp_1'}, use_global_device_ids=true, to_apply=%region_23.24 | all-reduce | flops 768 | bytes 6144 | tf_op jit(solution)/shard_map/psum | solution.py:49
  278.4 0.1 add_convert_fusion
  278.6 0.8 copy.20
  (57 shorter events, 0.9 us)
Async XLA Ops:
  2.4 7.6 %copy-start = (s32[384]{0:T(512)S(1)}, s32[384]{0:T(512)}, u32[]{:S(2)}) copy-start(s32[384]{0:T(512)} %param.11) | copy-start | bytes 4612
  2.4 12.0 %copy-start.1 = (bf16[3,31,128]{2,1,0:T(8,128)(2,1)S(1)}, bf16[3,31,128]{2,1,0:T(8,128)(2,1)}, u32[]{:S(2)}) copy-start(bf16[3,31,128]{2,1,0:T(8,128)(2,1)} %param.14) | copy-start | bytes 71428
  2.4 12.1 %copy-start.2 = (f32[3,2048]{1,0:T(4,128)S(1)}, f32[3,2048]{1,0:T(4,128)}, u32[]{:S(2)}) copy-start(f32[3,2048]{1,0:T(4,128)} %param.19) | copy-start | bytes 73732
  2.4 29.1 %all-to-all-start = ((bf16[16,384,128]{1,2,0:T(8,128)(2,1)}), bf16[16,384,128]{1,2,0:T(8,128)(2,1)S(1)}, u32[]{:S(2)}, u32[]{:S(2)}) async-start(bf16[16,384,128]{1,2,0:T(8,128)(2,1)} %broadcast_in_dim.12), calls=%async_computation | async-start | bytes 3145728 | tf_op jit(solution)/shard_map/all_to_all | solution.py:25
  10.1 4.5 %collective-permute-start.3 = (s32[15]{0:T(128)S(1)}, s32[15]{0:T(128)S(1)}, u32[]{:S(2)}, u32[]{:S(2)}) collective-permute-start(s32[15]{0:T(128)S(1)} %get-tuple-element.174), channel_id=1, source_target_pairs={{16,0},{32,16},{48,32},{64,48},{80,64},{96,80},{112,96},{128,112},... | collective-permute-start | bytes 188 | tf_op jit(solution)/shard_map/ppermute | solution.py:42
  12.0 4.9 %collective-permute-start.2 = (s32[15]{0:T(128)S(1)}, s32[15]{0:T(128)S(1)}, u32[]{:S(2)}, u32[]{:S(2)}) collective-permute-start(s32[15]{0:T(128)S(1)} %get-tuple-element.173), channel_id=1, source_target_pairs={{0,16},{16,32},{32,48},{48,64},{64,80},{80,96},{96,112},{112,128},... | collective-permute-start | bytes 188 | tf_op jit(solution)/shard_map/ppermute | solution.py:39
  34.9 5.7 %collective-permute-start = (bf16[15,128]{1,0:T(8,128)(2,1)S(1)}, bf16[15,128]{1,0:T(8,128)(2,1)S(1)}, u32[]{:S(2)}, u32[]{:S(2)}) collective-permute-start(bf16[15,128]{1,0:T(8,128)(2,1)S(1)} %get-tuple-element.27), channel_id=1, source_target_pairs={{0,16},{16,32},{32,48},{48,64},{64,80},{80,96},{96,112},{112,128},... | collective-permute-start | bytes 11528 | tf_op jit(solution)/shard_map/ppermute | solution.py:39
  36.8 5.8 %collective-permute-start.1 = (bf16[15,128]{1,0:T(8,128)(2,1)S(1)}, bf16[15,128]{1,0:T(8,128)(2,1)S(1)}, u32[]{:S(2)}, u32[]{:S(2)}) collective-permute-start(bf16[15,128]{1,0:T(8,128)(2,1)S(1)} %get-tuple-element.28), channel_id=1, source_target_pairs={{16,0},{32,16},{48,32},{64,48},{80,64},{96,80},{112,96},{128,112},... | collective-permute-start | bytes 11528 | tf_op jit(solution)/shard_map/ppermute | solution.py:42
  46.3 6.8 %copy-start.3 = (f32[3,2048]{1,0:T(4,128)S(1)}, f32[3,2048]{1,0:T(4,128)}, u32[]{:S(2)}) copy-start(f32[3,2048]{1,0:T(4,128)} %param.18) | copy-start | bytes 73732
  46.3 6.8 %copy-start.4 = (f32[3,2048]{1,0:T(4,128)S(1)}, f32[3,2048]{1,0:T(4,128)}, u32[]{:S(2)}) copy-start(f32[3,2048]{1,0:T(4,128)} %param.15) | copy-start | bytes 73732
  46.3 6.8 %copy-start.5 = (f32[3,2048]{1,0:T(4,128)S(1)}, f32[3,2048]{1,0:T(4,128)}, u32[]{:S(2)}) copy-start(f32[3,2048]{1,0:T(4,128)} %param.16) | copy-start | bytes 73732
  46.3 27.3 %all-to-all-start.1 = ((bf16[16,384,128]{1,2,0:T(8,128)(2,1)}), bf16[16,384,128]{1,2,0:T(8,128)(2,1)S(1)}, u32[]{:S(2)}, u32[]{:S(2)}) async-start(bf16[16,384,128]{1,2,0:T(8,128)(2,1)} %broadcast_in_dim.13), calls=%async_computation.1 | async-start | bytes 3145728 | tf_op jit(solution)/shard_map/all_to_all | solution.py:25
  97.2 24.6 %copy-start.6 = (bf16[3,2048,128]{2,1,0:T(8,128)(2,1)S(1)}, bf16[3,2048,128]{2,1,0:T(8,128)(2,1)}, u32[]{:S(2)}) copy-start(bf16[3,2048,128]{2,1,0:T(8,128)(2,1)} %param.12) | copy-start | bytes 4718596
  97.2 24.6 %all-to-all-start.2 = ((bf16[16,384,128]{1,2,0:T(8,128)(2,1)}), bf16[16,384,128]{1,2,0:T(8,128)(2,1)S(1)}, u32[]{:S(2)}, u32[]{:S(2)}) async-start(bf16[16,384,128]{1,2,0:T(8,128)(2,1)} %broadcast_in_dim.14), calls=%async_computation.2 | async-start | bytes 3145728 | tf_op jit(solution)/shard_map/all_to_all | solution.py:25
  124.1 5.6 %collective-permute-start.4 = (bf16[15,128]{1,0:T(8,128)(2,1)S(1)}, bf16[15,128]{1,0:T(8,128)(2,1)S(1)}, u32[]{:S(2)}, u32[]{:S(2)}) collective-permute-start(bf16[15,128]{1,0:T(8,128)(2,1)S(1)} %get-tuple-element.25), channel_id=1, source_target_pairs={{0,16},{16,32},{32,48},{48,64},{64,80},{80,96},{96,112},{112,128},... | collective-permute-start | bytes 11528 | tf_op jit(solution)/shard_map/ppermute | solution.py:39
  126.0 10.6 %collective-permute-start.5 = (bf16[15,128]{1,0:T(8,128)(2,1)S(1)}, bf16[15,128]{1,0:T(8,128)(2,1)S(1)}, u32[]{:S(2)}, u32[]{:S(2)}) collective-permute-start(bf16[15,128]{1,0:T(8,128)(2,1)S(1)} %get-tuple-element.26), channel_id=1, source_target_pairs={{16,0},{32,16},{48,32},{64,48},{80,64},{96,80},{112,96},{128,112},... | collective-permute-start | bytes 11528 | tf_op jit(solution)/shard_map/ppermute | solution.py:42
  187.1 24.1 %all-to-all-start.4 = ((bf16[16,384,128]{1,2,0:T(8,128)(2,1)}), bf16[16,384,128]{1,2,0:T(8,128)(2,1)S(1)}, u32[]{:S(2)}, u32[]{:S(2)}) async-start(bf16[16,384,128]{1,2,0:T(8,128)(2,1)} %broadcast_in_dim.16), calls=%async_computation.4 | async-start | bytes 3145728 | tf_op jit(solution)/shard_map/all_to_all | solution.py:25
  213.6 5.6 %collective-permute-start.6 = (bf16[15,128]{1,0:T(8,128)(2,1)S(1)}, bf16[15,128]{1,0:T(8,128)(2,1)S(1)}, u32[]{:S(2)}, u32[]{:S(2)}) collective-permute-start(bf16[15,128]{1,0:T(8,128)(2,1)S(1)} %get-tuple-element.23), channel_id=1, source_target_pairs={{0,16},{16,32},{32,48},{48,64},{64,80},{80,96},{96,112},{112,128},... | collective-permute-start | bytes 11528 | tf_op jit(solution)/shard_map/ppermute | solution.py:39
  215.5 5.0 %collective-permute-start.7 = (bf16[15,128]{1,0:T(8,128)(2,1)S(1)}, bf16[15,128]{1,0:T(8,128)(2,1)S(1)}, u32[]{:S(2)}, u32[]{:S(2)}) collective-permute-start(bf16[15,128]{1,0:T(8,128)(2,1)S(1)} %get-tuple-element.24), channel_id=1, source_target_pairs={{16,0},{32,16},{48,32},{64,48},{80,64},{96,80},{112,96},{128,112},... | collective-permute-start | bytes 11528 | tf_op jit(solution)/shard_map/ppermute | solution.py:42
  224.1 29.8 %all-to-all-start.5 = ((bf16[16,384,128]{1,2,0:T(8,128)(2,1)}), bf16[16,384,128]{1,2,0:T(8,128)(2,1)S(1)}, u32[]{:S(2)}, u32[]{:S(2)}) async-start(bf16[16,384,128]{1,2,0:T(8,128)(2,1)} %broadcast_in_dim.17), calls=%async_computation.5 | async-start | bytes 3145728 | tf_op jit(solution)/shard_map/all_to_all | solution.py:25
where the time goes:
time: 281 us; the launch traced here: 279 us
  waiting for transfers between devices  112 us (40%)
  blocking collectives  82.2 us (29%)
  starting transfers between devices  49.2 us (18%)
  other arithmetic  13.6 us (5%)
  matrix products  12.6 us (4%)
  local copies, waits for them, and re-layouts  9.45 us (3%)
    all_to_all x5, waiting for transfers between devices, from_everyone(): lax.all_to_all(jnp.broadcast_to(array[None], (devices, *array.shape)), ax...  99.3 us
    psum x6, blocking collectives, by_axis(): array = lax.psum(array, axis)  57.3 us
    all_to_all x5, starting transfers between devices, from_everyone(): lax.all_to_all(jnp.broadcast_to(array[None], (devices, *array.shape)), ax...  28.2 us
    all_to_all x1, blocking collectives, from_everyone(): lax.all_to_all(jnp.broadcast_to(array[None], (devices, *array.shape)), ax...  24.9 us
    ppermute x4, starting transfers between devices, padded(): lax.ppermute(lax.slice_in_dim(block, 0, width, axis=dim), axis, backward)  12.8 us
    ppermute x4, waiting for transfers between devices, padded(): lax.ppermute(lax.slice_in_dim(block, 0, width, axis=dim), axis, backward)  10.2 us
    ppermute x4, starting transfers between devices, padded(): lax.ppermute(lax.slice_in_dim(block, block.shape[dim] - width, None, axis...  8.17 us
    dot_general x6, matrix products, add_product(): return jnp.dot(piece, weight, preferred_element_type=jnp.float32)  7.94 us
  transfers between devices with their start and end apart: 13, of which 9 were waited for; matrix products, arithmetic and copies ran while one was open for 0% of the time, Pallas kernels for 0%

commit v1 on v0

v1 whole, which is shorter than its diff:
```python
import functools

import jax
import jax.numpy as jnp
from jax import lax
from jax.experimental import pallas as pl
from jax.experimental.pallas import tpu as pltpu
from jax.sharding import PartitionSpec as P

LAYERS = 3
KERNEL = 31
HALF = 15
PAD = 16
LANES = 128
SIDE = 4
PEERS = SIDE * SIDE
ALPHA = 2.0**0.25
EPS = 1e-05
MESH = pl.DeviceIdType.MESH


class Tree:
    def __init__(self, env, gather, piece, row0, rows, x_first, up):
        self.env, self.g, self.p = env, gather, piece
        self.row0, self.rows, self.x_first, self.up = row0, rows, x_first, up

    def block(self, du, dv):
        dx, dy = (du, dv) if self.x_first else (dv, du)
        e = self.env
        slot = lax.rem(e["y"] + dy + SIDE, SIDE) * SIDE + lax.rem(e["x"] + dx + SIDE, SIDE)
        return e["gbuf"].at[self.g, slot, pl.ds(self.row0, self.rows), :]

    def copy(self, du, dv, eu, ev):
        e = self.env
        ex, ey = (eu, ev) if self.x_first else (ev, eu)
        peer = lax.rem(e["y"] + ey + SIDE, SIDE) * SIDE + lax.rem(e["x"] + ex + SIDE, SIDE)
        there = ((du - eu) % SIDE) * SIDE + (dv - ev) % SIDE
        ref = self.block(du, dv)
        return pltpu.make_async_remote_copy(
            src_ref=ref,
            dst_ref=ref,
            send_sem=e["send"].at[self.g, self.p, there],
            recv_sem=e["recv"].at[self.g, self.p, there],
            device_id=(e["s"], peer),
            device_id_type=MESH,
        )

    def sends(self):
        up = 1 if self.up else -1
        out = {(0, 0): [(1, 0), (-1, 0), (0, 1), (0, -1)]}
        for du in (-1, 1, 2):
            out[(du, 0)] = [(0, 1), (0, -1)]
        out[(-up, 0)].insert(0, (up, 0))
        for du in (0, 1, -1, 2):
            forward = up if du in (0, 2) else -up
            out[(du, -forward)] = [(0, forward)]
        return out

    def order(self):
        first = [(-1, 0), (1, 0)] if self.up else [(1, 0), (-1, 0)]
        return first + [(0, -1), (0, 1), (2, 0), (-1, -1), (-1, 1), (1, -1), (1, 1), (2, -1), (2, 1)] + [
            (0, 2), (-1, 2), (1, 2), (2, 2)
        ]

    def start(self):
        for eu, ev in self.sends()[(0, 0)]:
            self.copy(0, 0, eu, ev).start()

    def arrive(self, du, dv):
        index = (du % SIDE) * SIDE + dv % SIDE
        e = self.env
        ref = self.block(du, dv)
        pltpu.make_async_remote_copy(
            src_ref=ref,
            dst_ref=ref,
            send_sem=e["send"].at[self.g, self.p, index],
            recv_sem=e["recv"].at[self.g, self.p, index],
            device_id=(e["s"], e["y"] * SIDE + e["x"]),
            device_id_type=MESH,
        ).wait_recv()
        for eu, ev in self.sends().get((du, dv), []):
            self.copy(du, dv, eu, ev).start()

    def drain(self):
        for (du, dv), targets in self.sends().items():
            for eu, ev in targets:
                self.copy(du, dv, eu, ev).wait_send()


def gather_all(trees):
    for step in range(len(trees[0].order())):
        for tree in trees:
            tree.arrive(*tree.order()[step])


def column(row):
    return jnp.swapaxes(jnp.broadcast_to(row, (LANES, LANES)), 0, 1)


def kernel(
    ns,
    stream, doc, wv, wg, ck, cg, cs, wp, og, osh,
    out,
    gbuf, wvg, wpb, ckv, cgv, csv, ogv, osv, docv, docs, nleft, nright, glu, hsend, hrecv, act, keep, z32, stat,
    stsend, strecv,
    load, send, recv, hss, hrs, dss, drs, ss, sr,
):
    rows = stream.shape[0]
    s = lax.axis_index("sp")
    t = lax.axis_index("tp")
    y, x = t // SIDE, t % SIDE
    env = dict(s=s, x=x, y=y, gbuf=gbuf, send=send, recv=recv)
    after, before = lax.rem(s + 1, ns), lax.rem(s + ns - 1, ns)

    loads = [pltpu.make_async_copy(stream, gbuf.at[0, t], load.at[0])]
    loads.append(pltpu.make_async_copy(doc, docv, load.at[1]))
    for n, (src, dst) in enumerate(((ck, ckv), (cg, cgv), (cs, csv), (og, ogv), (osh, osv))):
        loads.append(pltpu.make_async_copy(src, dst, load.at[2 + n]))
    weights = []
    for layer in range(LAYERS):
        weights.append([
            pltpu.make_async_copy(wv.at[layer], wvg.at[layer, :, pl.ds(0, LANES)], load.at[7 + 3 * layer]),
            pltpu.make_async_copy(wg.at[layer], wvg.at[layer, :, pl.ds(LANES, LANES)], load.at[8 + 3 * layer]),
            pltpu.make_async_copy(wp.at[layer], wpb.at[layer], load.at[9 + 3 * layer]),
        ])
    for c in loads:
        c.start()
    for group in weights:
        for c in group:
            c.start()

    barrier = pltpu.get_barrier_semaphore()
    for d in range(1, PEERS):
        pl.semaphore_signal(barrier, inc=1, device_id=(s, lax.rem(t + d, PEERS)), device_id_type=MESH)
    for other in (after, before):
        pl.semaphore_signal(barrier, inc=1, device_id=(other, t), device_id_type=MESH)
    loads[0].wait()
    pl.semaphore_wait(barrier, PEERS + 1)

    quarter = rows // 4

    def trees_of(g):
        return [Tree(env, g, p, p * quarter, quarter, p % 2 == 0, p < 2) for p in range(4)]

    def halo(src, dst, sem_s, sem_r, who):
        return pltpu.make_async_remote_copy(
            src_ref=src, dst_ref=dst, send_sem=sem_s, recv_sem=sem_r, device_id=(who, t), device_id_type=MESH
        )

    trees = trees_of(0)
    for tree in trees:
        tree.start()

    loads[1].wait()
    for n in range(rows // LANES):
        docs[PAD + n * LANES : PAD + (n + 1) * LANES, :] = column(
            docv[0:1, n * LANES : (n + 1) * LANES].astype(jnp.float32)
        )
    right_doc = halo(docs.at[pl.ds(rows, PAD)], docs.at[pl.ds(0, PAD)], dss.at[0], drs.at[0], after)
    left_doc = halo(docs.at[pl.ds(PAD, PAD)], docs.at[pl.ds(rows + PAD, PAD)], dss.at[1], drs.at[1], before)
    right_doc.start()
    left_doc.start()
    for c in loads[2:]:
        c.wait()
    for group in weights:
        for c in group:
            c.wait()
    right_doc.wait()
    left_doc.wait()

    @pl.when(s == 0)
    def _():
        docs[0:PAD, :] = jnp.full((PAD, LANES), -1.0, jnp.float32)

    @pl.when(s == ns - 1)
    def _():
        docs[rows + PAD : rows + 2 * PAD, :] = jnp.full((PAD, LANES), -1.0, jnp.float32)

    def reach(n, carry):
        base = pl.multiple_of(n * PAD, PAD)
        mine = docs[pl.ds(base + PAD, PAD), :]
        low = jnp.zeros((PAD, LANES), jnp.float32)
        high = jnp.zeros((PAD, LANES), jnp.float32)
        for j in range(1, HALF + 1):
            low = low + (docs[pl.ds(base + PAD - j, PAD), :] == mine).astype(jnp.float32)
            high = high + (docs[pl.ds(base + PAD + j, PAD), :] == mine).astype(jnp.float32)
        nleft[pl.ds(base, PAD), :] = low
        nright[pl.ds(base, PAD), :] = high
        return carry

    lax.fori_loop(0, rows // PAD, reach, 0)

    def conv_tile(layer, base):
        low = nleft[pl.ds(base, PAD), :]
        high = nright[pl.ds(base, PAD), :]
        taps = ckv[layer].astype(jnp.float32)
        total = glu[pl.ds(base + PAD, PAD), :] * taps[HALF : HALF + 1, :]
        for j in range(1, HALF + 1):
            a = glu[pl.ds(base + PAD - j, PAD), :]
            b = glu[pl.ds(base + PAD + j, PAD), :]
            total = total + jnp.where(low >= j, a, 0.0) * taps[HALF - j : HALF - j + 1, :]
            total = total + jnp.where(high >= j, b, 0.0) * taps[HALF + j : HALF + j + 1, :]
        gbuf[2 * layer + 1, t, pl.ds(base, PAD), :] = total.astype(jnp.bfloat16)

    group = 96

    def normed(g, layer, gain, shift, silu):
        def body(n, carry):
            base = pl.multiple_of(n * group, 32)
            one = jnp.zeros((group, LANES), jnp.float32)
            two = jnp.zeros((group, LANES), jnp.float32)
            for j in range(PEERS):
                v = gbuf[g, j, pl.ds(base, group), :].astype(jnp.float32)
                one = one + v
                two = two + v * v
            width = PEERS * LANES
            mean = jnp.sum(one, axis=1, keepdims=True) * (1.0 / width)
            var = jnp.maximum(jnp.sum(two, axis=1, keepdims=True) * (1.0 / width) - mean * mean, 0.0)
            scale = lax.rsqrt(var + EPS)
            for j in range(PEERS):
                v = gbuf[g, j, pl.ds(base, group), :].astype(jnp.float32)
                cols = slice(j * LANES, (j + 1) * LANES)
                v = (v - mean) * scale * gain[layer : layer + 1, cols] + shift[layer : layer + 1, cols]
                if silu:
                    v = v / (1.0 + jnp.exp(-v))
                act[j, pl.ds(base, group), :] = v.astype(jnp.bfloat16)
            return carry

        lax.fori_loop(0, rows // group, body, 0)

    half = rows // 2
    for layer in range(LAYERS):
        g = 2 * layer
        gather_all(trees)
        if layer == 0:
            keep[...] = gbuf[0, t].astype(jnp.float32)
        else:
            normed(g, layer - 1, ogv, osv, False)
            keep[...] = act[t].astype(jnp.float32)
        for h in range(2):
            part = slice(h * half, (h + 1) * half)
            if layer == 0:
                lhs = jnp.concatenate([gbuf[0, j, part, :] for j in range(PEERS)], axis=1)
            else:
                lhs = jnp.concatenate([act[j, part, :] for j in range(PEERS)], axis=1)
            both = jnp.dot(lhs, wvg[layer], preferred_element_type=jnp.float32)
            lin, gat = both[:, :LANES], both[:, LANES:]
            value = (lin / (1.0 + jnp.exp(-gat))).astype(jnp.bfloat16)
            glu[PAD + h * half : PAD + (h + 1) * half, :] = value.astype(jnp.float32)
            if h == 0:
                hsend[layer, 0] = value[:PAD]
            else:
                hsend[layer, 1] = value[half - PAD :]
        right = halo(hsend.at[layer, 1], hrecv.at[layer, 0], hss.at[layer, 0], hrs.at[layer, 0], after)
        left = halo(hsend.at[layer, 0], hrecv.at[layer, 1], hss.at[layer, 1], hrs.at[layer, 1], before)
        right.start()
        left.start()
        for tree in trees:
            tree.drain()

        def inner(n, carry):
            conv_tile(layer, pl.multiple_of(n * PAD, PAD))
            return carry

        lax.fori_loop(1, rows // PAD - 1, inner, 0)
        right.wait()
        left.wait()
        glu[0:PAD, :] = hrecv[layer, 0].astype(jnp.float32)
        glu[rows + PAD : rows + 2 * PAD, :] = hrecv[layer, 1].astype(jnp.float32)
        conv_tile(layer, 0)
        conv_tile(layer, rows - PAD)

        trees = trees_of(g + 1)
        for tree in trees:
            tree.start()
        gather_all(trees)
        normed(g + 1, layer, cgv, csv, True)
        for h in range(2):
            part = slice(h * half, (h + 1) * half)
            lhs = jnp.concatenate([act[j, part, :] for j in range(PEERS)], axis=1)
            z = ALPHA * keep[part, :] + jnp.dot(lhs, wpb[layer], preferred_element_type=jnp.float32)
            if layer < LAYERS - 1:
                gbuf[g + 2, t, part, :] = z.astype(jnp.bfloat16)
            else:
                z32[part, :] = z
        for tree in trees:
            tree.drain()
        if layer < LAYERS - 1:
            trees = trees_of(g + 2)
            for tree in trees:
                tree.start()

    ones = jnp.ones((8, LANES), jnp.float32)
    z = z32[...]
    contract = (((1,), (1,)), ((), ()))
    one = lax.dot_general(ones, z, contract, precision=lax.Precision.HIGHEST, preferred_element_type=jnp.float32)
    two = lax.dot_general(ones, z * z, contract, precision=lax.Precision.HIGHEST, preferred_element_type=jnp.float32)
    stsend[0:1, :] = one[0:1, :]
    stsend[1:2, :] = two[0:1, :]
    outgoing = []
    for d in range(1, PEERS):
        c = pltpu.make_async_remote_copy(
            src_ref=stsend,
            dst_ref=strecv.at[d],
            send_sem=ss.at[d],
            recv_sem=sr.at[d],
            device_id=(s, lax.rem(t + d, PEERS)),
            device_id_type=MESH,
        )
        c.start()
        outgoing.append(c)
    sums = stsend[...]
    for d in range(1, PEERS):
        outgoing[d - 1].wait_recv()
        sums = sums + strecv[d]
    stat[...] = sums
    mine = pl.ds(pl.multiple_of(t * LANES, LANES), LANES)
    gain = ogv[LAYERS - 1 : LAYERS, mine]
    shift = osv[LAYERS - 1 : LAYERS, mine]
    width = PEERS * LANES
    for n in range(rows // LANES):
        cols = slice(n * LANES, (n + 1) * LANES)
        mean = column(stat[0:1, cols]) * (1.0 / width)
        var = jnp.maximum(column(stat[1:2, cols]) * (1.0 / width) - mean * mean, 0.0)
        v = (z32[cols, :] - mean) * lax.rsqrt(var + EPS) * gain + shift
        out[cols, :] = v.astype(jnp.bfloat16)
    for c in outgoing:
        c.wait_send()


def on_device(ns, stream, doc_ids, w_value, w_gate, conv_kernel, conv_gain, conv_shift, w_proj, out_gain, out_shift):
    rows, width = stream.shape[0], w_value.shape[1]
    gathers = 2 * LAYERS
    bf16, f32 = jnp.bfloat16, jnp.float32
    dma = pltpu.SemaphoreType.DMA
    return pl.pallas_call(
        functools.partial(kernel, ns),
        out_shape=jax.ShapeDtypeStruct((rows, LANES), bf16),
        in_specs=[pl.BlockSpec(memory_space=pl.ANY)] * 10,
        out_specs=pl.BlockSpec(memory_space=pltpu.VMEM),
        scratch_shapes=[
            pltpu.VMEM((gathers, PEERS, rows, LANES), bf16),
            pltpu.VMEM((LAYERS, width, 2 * LANES), bf16),
            pltpu.VMEM((LAYERS, width, LANES), bf16),
            pltpu.VMEM((LAYERS, KERNEL, LANES), bf16),
            pltpu.VMEM((LAYERS, width), f32),
            pltpu.VMEM((LAYERS, width), f32),
            pltpu.VMEM((LAYERS, width), f32),
            pltpu.VMEM((LAYERS, width), f32),
            pltpu.VMEM((1, rows), jnp.int32),
            pltpu.VMEM((rows + 2 * PAD, LANES), f32),
            pltpu.VMEM((rows, LANES), f32),
            pltpu.VMEM((rows, LANES), f32),
            pltpu.VMEM((rows + 2 * PAD, LANES), f32),
            pltpu.VMEM((LAYERS, 2, PAD, LANES), bf16),
            pltpu.VMEM((LAYERS, 2, PAD, LANES), bf16),
            pltpu.VMEM((PEERS, rows, LANES), bf16),
            pltpu.VMEM((rows, LANES), f32),
            pltpu.VMEM((rows, LANES), f32),
            pltpu.VMEM((2, rows), f32),
            pltpu.VMEM((2, rows), f32),
            pltpu.VMEM((PEERS, 2, rows), f32),
            dma((7 + 3 * LAYERS,)),
            dma((gathers, 4, PEERS)),
            dma((gathers, 4, PEERS)),
            dma((LAYERS, 2)),
            dma((LAYERS, 2)),
            dma((2,)),
            dma((2,)),
            dma((PEERS,)),
            dma((PEERS,)),
        ],
        compiler_params=pltpu.CompilerParams(
            collective_id=0, has_side_effects=True, vmem_limit_bytes=60 * 1024 * 1024
        ),
        name="stack",
    )(stream, doc_ids.reshape(1, rows), w_value, w_gate, conv_kernel, conv_gain, conv_shift, w_proj, out_gain, out_shift)


def solution(mesh):
    return jax.shard_map(
        functools.partial(on_device, mesh.shape["sp"]),
        mesh=mesh,
        in_specs=(
            P("sp", "tp"), P("sp"), P(None, None, "tp"), P(None, None, "tp"), P(None, None, "tp"), P(), P(),
            P(None, None, "tp"), P(), P(),
        ),
        out_specs=P("sp", "tp"),
        check_vma=False,
    )
```

time: 281 us -> 133 us (0.47)
  the two profiles are of different devices: /device:TPU:98 before, /device:TPU:2 now
where the time goes in v1:
time: 133 us
  Pallas kernels  130 us (98%)
  local copies, waits for them, and re-layouts  2.78 us (2%)
    pallas_call x1, Pallas kernels, on_device(): pl.pallas_call(functools.partial(kernel, ns), out_shape=jax.ShapeDtypeStr...  130 us

profile of v1, /device:TPU:2, one launch (start us, length us, event | category | flops | bytes accessed | tf_op | source)
XLA Modules:
  0.0 132.7 jit_solution(21590710931215139)
XLA Ops:
  0.0 1.2 reshape.3.doc
  1.2 129.9 %stack.1 = bf16[384,128]{1,0:T(8,128)(2,1)} custom-call(bf16[384,128]{1,0:T(8,128)(2,1)} %stream.1, s32[1,384]{1,0:T(1,128)} %reshape.3.doc, bf16[3,2048,128]{2,1,0:T(8,128)(2,1)} %wv.1, bf16[3,2048,128]{2,1,0:T(8,128)(2,1)} %wg.1, bf16[3,31,128]{2,1,0:T(8,128)(2,1)} %ck.1, f32[3,2048]{1,0:T(4,128)} %cg.1, f32[3,2048]{1,0:T(4,128)} %cs.1, ...), custom_call_target="tpu_custom_call" | custom-call | tf_op jit(solution)/shard_map/stack/pallas_call | solution.py:336
  131.2 1.5 %copy.12 = bf16[384,128]{1,0:T(8,128)(2,1)} copy(bf16[384,128]{1,0:T(8,128)(2,1)} %stack.1) | data formatting | bytes 196608

commit v2 on v1

v2 whole, which is shorter than its diff:
```python
import functools

import jax
import jax.numpy as jnp
from jax import lax
from jax.experimental import pallas as pl
from jax.experimental.pallas import tpu as pltpu
from jax.sharding import PartitionSpec as P

LAYERS = 3
KERNEL = 31
HALF = 15
PAD = 16
LANES = 128
SIDE = 4
PEERS = SIDE * SIDE
STEPS = (1, -1, 2)
CHUNKS = 3
OUTER = 80
MIDDLE = 144
ALPHA = 2.0**0.25
EPS = 1e-05
MESH = pl.DeviceIdType.MESH


class Spread:
    def __init__(self, env, stage, piece, row0, rows, x_first):
        self.env, self.k, self.p = env, stage, piece
        self.row0, self.rows, self.x_first = row0, rows, x_first

    def at(self, du, dv):
        dx, dy = (du, dv) if self.x_first else (dv, du)
        e = self.env
        return lax.rem(e["y"] + dy + SIDE, SIDE) * SIDE + lax.rem(e["x"] + dx + SIDE, SIDE)

    def ref(self, slot):
        return self.env["gbuf"].at[self.k, slot, pl.ds(self.row0, self.rows), :]

    def copy(self, src, dst, recv, peer):
        e = self.env
        return pltpu.make_async_remote_copy(
            src_ref=src,
            dst_ref=dst,
            send_sem=e["send"].at[self.k, self.p],
            recv_sem=e["recv"].at[self.k, self.p, recv],
            device_id=(e["s"], peer),
            device_id_type=MESH,
        )

    def spread(self, du):
        mine = self.ref(self.at(du, 0))
        for dv in (2, 1, -1):
            self.copy(mine, mine, 3, self.at(0, dv)).start()

    def start(self):
        mine = self.ref(self.at(0, 0))
        for n, du in enumerate(STEPS):
            self.copy(mine, mine, n, self.at(-du, 0)).start()
        self.spread(0)

    def turn(self):
        for n, du in enumerate(STEPS):
            block = self.ref(self.at(du, 0))
            self.copy(block, block, n, self.at(1, 0)).wait_recv()
            self.spread(du)

    def finish(self):
        many = self.ref(pl.ds(0, PEERS - SIDE))
        self.copy(many, many, 3, self.at(1, 0)).wait_recv()

    def drain(self):
        many = self.ref(pl.ds(0, PEERS - 1))
        self.copy(many, many, 3, self.at(1, 0)).wait_send()


def bounds(rows):
    outer, middle = OUTER, MIDDLE
    cuts = []
    for k in range(2 * LAYERS):
        lost = PAD * ((k + 1) // 2)
        cuts.append((0, outer - lost, middle - lost, rows // 2))
    return cuts


def plan(cuts):
    now, link, order = 0.0, 0.0, []
    ready = {("turn", c, 0): 3.0 + 0.5 * c for c in range(CHUNKS)}
    done = set()

    def rows_of(c, k):
        return 2 * (cuts[k][c + 1] - cuts[k][c])

    while ready:
        allowed = [
            step for step in ready
            if step[0] != "conv" or all(("finish", c, step[2]) in done for c in range(step[1]))
        ]
        step = min(allowed, key=lambda each: (max(ready[each], now), ready[each], each[1]))
        what, c, k = step
        now = max(now, ready.pop(step))
        order.append(step)
        done.add(step)
        if what == "turn":
            now += 0.15
            link = max(now + 3.0, link) + 0.02 * rows_of(c, k)
            ready["finish", c, k] = link
        elif what == "finish" and k % 2 == 0:
            now += 0.4 + 0.005 * rows_of(c, k)
            ready["conv", c, k] = now + (2.5 if c == 0 else 0.0)
        elif what == "finish":
            now += 0.4 + 0.008 * rows_of(c, k)
            if k + 1 < 2 * LAYERS:
                ready["turn", c, k + 1] = now + 3.0
        else:
            now += 0.2 + 0.003 * rows_of(c, k)
            ready["turn", c, k + 1] = now + 3.0
    return order


def column(row):
    return jnp.swapaxes(jnp.broadcast_to(row, (LANES, LANES)), 0, 1)


def kernel(
    ns,
    stream, doc, wv, wg, ck, cg, cs, wp, og, osh,
    out,
    gbuf, wvg, wpb, ckv, cgv, csv, ogv, osv, docv, docs, nleft, nright, glu, hsend, hrecv, act, keep, z32, stat,
    stsend, strecv,
    load, send, recv, hss, hrs, dss, drs, ss, sr,
):
    rows = stream.shape[0]
    s = lax.axis_index("sp")
    t = lax.axis_index("tp")
    y, x = t // SIDE, t % SIDE
    env = dict(s=s, x=x, y=y, gbuf=gbuf, send=send, recv=recv)
    after, before = lax.rem(s + 1, ns), lax.rem(s + ns - 1, ns)

    loads = [pltpu.make_async_copy(stream, gbuf.at[0, t], load.at[0])]
    loads.append(pltpu.make_async_copy(doc, docv, load.at[1]))
    for n, (src, dst) in enumerate(((ck, ckv), (cg, cgv), (cs, csv), (og, ogv), (osh, osv))):
        loads.append(pltpu.make_async_copy(src, dst, load.at[2 + n]))
    weights = []
    for layer in range(LAYERS):
        weights.append([
            pltpu.make_async_copy(wv.at[layer], wvg.at[layer, :, pl.ds(0, LANES)], load.at[7 + 3 * layer]),
            pltpu.make_async_copy(wg.at[layer], wvg.at[layer, :, pl.ds(LANES, LANES)], load.at[8 + 3 * layer]),
            pltpu.make_async_copy(wp.at[layer], wpb.at[layer], load.at[9 + 3 * layer]),
        ])
    for c in loads:
        c.start()
    for group in weights:
        for c in group:
            c.start()

    barrier = pltpu.get_barrier_semaphore()
    for d in range(1, PEERS):
        pl.semaphore_signal(barrier, inc=1, device_id=(s, lax.rem(t + d, PEERS)), device_id_type=MESH)
    for other in (after, before):
        pl.semaphore_signal(barrier, inc=1, device_id=(other, t), device_id_type=MESH)
    loads[0].wait()
    pl.semaphore_wait(barrier, PEERS + 1)

    cuts = bounds(rows)
    pieces = {}
    for k in range(2 * LAYERS):
        for c in range(CHUNKS):
            low, high = cuts[k][c], cuts[k][c + 1]
            pieces[c, k] = (
                Spread(env, k, 2 * c, low, high - low, True),
                Spread(env, k, 2 * c + 1, rows - high, high - low, False),
            )

    def start(c, k):
        for piece in pieces[c, k]:
            piece.start()

    def halo(src, dst, sem_s, sem_r, who):
        return pltpu.make_async_remote_copy(
            src_ref=src, dst_ref=dst, send_sem=sem_s, recv_sem=sem_r, device_id=(who, t), device_id_type=MESH
        )

    for c in range(CHUNKS):
        start(c, 0)

    loads[1].wait()
    for n in range(rows // LANES):
        docs[PAD + n * LANES : PAD + (n + 1) * LANES, :] = column(
            docv[0:1, n * LANES : (n + 1) * LANES].astype(jnp.float32)
        )
    right_doc = halo(docs.at[pl.ds(rows, PAD)], docs.at[pl.ds(0, PAD)], dss.at[0], drs.at[0], after)
    left_doc = halo(docs.at[pl.ds(PAD, PAD)], docs.at[pl.ds(rows + PAD, PAD)], dss.at[1], drs.at[1], before)
    right_doc.start()
    left_doc.start()
    for c in loads[2:]:
        c.wait()
    for group in weights:
        for c in group:
            c.wait()
    right_doc.wait()
    left_doc.wait()

    @pl.when(s == 0)
    def _():
        docs[0:PAD, :] = jnp.full((PAD, LANES), -1.0, jnp.float32)

    @pl.when(s == ns - 1)
    def _():
        docs[rows + PAD : rows + 2 * PAD, :] = jnp.full((PAD, LANES), -1.0, jnp.float32)

    def reach(n, carry):
        base = pl.multiple_of(n * PAD, PAD)
        mine = docs[pl.ds(base + PAD, PAD), :]
        low = jnp.zeros((PAD, LANES), jnp.float32)
        high = jnp.zeros((PAD, LANES), jnp.float32)
        for j in range(1, HALF + 1):
            low = low + (docs[pl.ds(base + PAD - j, PAD), :] == mine).astype(jnp.float32)
            high = high + (docs[pl.ds(base + PAD + j, PAD), :] == mine).astype(jnp.float32)
        nleft[pl.ds(base, PAD), :] = low
        nright[pl.ds(base, PAD), :] = high
        return carry

    lax.fori_loop(0, rows // PAD, reach, 0)

    def conv_rows(layer, first, last):
        def tile(n, carry):
            base = pl.multiple_of(n * PAD, PAD)
            low = nleft[pl.ds(base, PAD), :]
            high = nright[pl.ds(base, PAD), :]
            taps = ckv[layer].astype(jnp.float32)
            total = glu[layer, pl.ds(base + PAD, PAD), :] * taps[HALF : HALF + 1, :]
            for j in range(1, HALF + 1):
                a = glu[layer, pl.ds(base + PAD - j, PAD), :]
                b = glu[layer, pl.ds(base + PAD + j, PAD), :]
                total = total + jnp.where(low >= j, a, 0.0) * taps[HALF - j : HALF - j + 1, :]
                total = total + jnp.where(high >= j, b, 0.0) * taps[HALF + j : HALF + j + 1, :]
            gbuf[2 * layer + 1, t, pl.ds(base, PAD), :] = total.astype(jnp.bfloat16)
            return carry

        lax.fori_loop(first // PAD, last // PAD, tile, 0)

    def normed(k, layer, gain, shift, silu, part):
        count = part.stop - part.start
        one = jnp.zeros((count, LANES), jnp.float32)
        two = jnp.zeros((count, LANES), jnp.float32)
        for j in range(PEERS):
            v = gbuf[k, j, part, :].astype(jnp.float32)
            one = one + v
            two = two + v * v
        width = PEERS * LANES
        mean = jnp.sum(one, axis=1, keepdims=True) * (1.0 / width)
        var = jnp.maximum(jnp.sum(two, axis=1, keepdims=True) * (1.0 / width) - mean * mean, 0.0)
        scale = lax.rsqrt(var + EPS)
        for j in range(PEERS):
            v = gbuf[k, j, part, :].astype(jnp.float32)
            cols = slice(j * LANES, (j + 1) * LANES)
            v = (v - mean) * scale * gain[layer : layer + 1, cols] + shift[layer : layer + 1, cols]
            if silu:
                v = v / (1.0 + jnp.exp(-v))
            act[j, part, :] = v.astype(jnp.bfloat16)

    def halos(layer):
        return [
            halo(hsend.at[layer, 1], hrecv.at[layer, 0], hss.at[layer, 0], hrs.at[layer, 0], after),
            halo(hsend.at[layer, 0], hrecv.at[layer, 1], hss.at[layer, 1], hrs.at[layer, 1], before),
        ]

    def sides(c, k):
        return [slice(p.row0, p.row0 + p.rows) for p in pieces[c, k]]

    def joined(ref, parts):
        rows_of = [jnp.concatenate([ref[j, part, :] for j in range(PEERS)], axis=1) for part in parts]
        return jnp.concatenate(rows_of, axis=0)

    def gated(c, k):
        layer, parts = k // 2, sides(c, k)
        if layer == 0:
            lhs = joined(gbuf.at[0], parts)
            for part in parts:
                keep[part, :] = gbuf[0, t, part, :].astype(jnp.float32)
        else:
            for part in parts:
                normed(k, layer - 1, ogv, osv, False, part)
                keep[part, :] = act[t, part, :].astype(jnp.float32)
            lhs = joined(act, parts)
        both = jnp.dot(lhs, wvg[layer], preferred_element_type=jnp.float32)
        value = (both[:, :LANES] / (1.0 + jnp.exp(-both[:, LANES:]))).astype(jnp.bfloat16)
        count = pieces[c, k][0].rows
        for n, part in enumerate(parts):
            mine = value[n * count : (n + 1) * count]
            glu[layer, PAD + part.start : PAD + part.stop, :] = mine.astype(jnp.float32)
            if c == 0:
                hsend[layer, n] = mine[:PAD] if n == 0 else mine[count - PAD :]
        if c == 0:
            for h in halos(layer):
                h.start()

    def convolved(c, k):
        layer = k // 2
        left, right = sides(c, k + 1)
        if c == 0:
            conv_rows(layer, left.start + PAD, left.stop)
            conv_rows(layer, right.start, right.stop - PAD)
            for h in halos(layer):
                h.wait()
            glu[layer, 0:PAD, :] = hrecv[layer, 0].astype(jnp.float32)
            glu[layer, rows + PAD : rows + 2 * PAD, :] = hrecv[layer, 1].astype(jnp.float32)
            conv_rows(layer, 0, PAD)
            conv_rows(layer, rows - PAD, rows)
        elif left.stop == right.start:
            conv_rows(layer, left.start, right.stop)
        else:
            conv_rows(layer, left.start, left.stop)
            conv_rows(layer, right.start, right.stop)

    def projected(c, k):
        layer, parts = k // 2, sides(c, k)
        for part in parts:
            normed(k, layer, cgv, csv, True, part)
        branch = jnp.dot(joined(act, parts), wpb[layer], preferred_element_type=jnp.float32)
        count = pieces[c, k][0].rows
        for n, part in enumerate(parts):
            z = ALPHA * keep[part, :] + branch[n * count : (n + 1) * count]
            if layer < LAYERS - 1:
                gbuf[k + 1, t, part, :] = z.astype(jnp.bfloat16)
            else:
                z32[part, :] = z

    for what, c, k in plan(cuts):
        if what == "turn":
            for piece in pieces[c, k]:
                piece.turn()
        elif what == "finish":
            for piece in pieces[c, k]:
                piece.finish()
            if k % 2 == 0:
                gated(c, k)
            else:
                projected(c, k)
                if k + 1 < 2 * LAYERS:
                    start(c, k + 1)
        else:
            convolved(c, k)
            start(c, k + 1)

    ones = jnp.ones((8, LANES), jnp.float32)
    z = z32[...]
    contract = (((1,), (1,)), ((), ()))
    one = lax.dot_general(ones, z, contract, precision=lax.Precision.HIGHEST, preferred_element_type=jnp.float32)
    two = lax.dot_general(ones, z * z, contract, precision=lax.Precision.HIGHEST, preferred_element_type=jnp.float32)
    stsend[0:1, :] = one[0:1, :]
    stsend[1:2, :] = two[0:1, :]
    outgoing = []
    for d in range(1, PEERS):
        c = pltpu.make_async_remote_copy(
            src_ref=stsend,
            dst_ref=strecv.at[d],
            send_sem=ss.at[d],
            recv_sem=sr.at[d],
            device_id=(s, lax.rem(t + d, PEERS)),
            device_id_type=MESH,
        )
        c.start()
        outgoing.append(c)
    sums = stsend[...]
    for d in range(1, PEERS):
        outgoing[d - 1].wait_recv()
        sums = sums + strecv[d]
    stat[...] = sums
    mine = pl.ds(pl.multiple_of(t * LANES, LANES), LANES)
    gain = ogv[LAYERS - 1 : LAYERS, mine]
    shift = osv[LAYERS - 1 : LAYERS, mine]
    width = PEERS * LANES
    for n in range(rows // LANES):
        cols = slice(n * LANES, (n + 1) * LANES)
        mean = column(stat[0:1, cols]) * (1.0 / width)
        var = jnp.maximum(column(stat[1:2, cols]) * (1.0 / width) - mean * mean, 0.0)
        v = (z32[cols, :] - mean) * lax.rsqrt(var + EPS) * gain + shift
        out[cols, :] = v.astype(jnp.bfloat16)
    for c in outgoing:
        c.wait_send()
    for pair in pieces.values():
        for piece in pair:
            piece.drain()


def on_device(ns, stream, doc_ids, w_value, w_gate, conv_kernel, conv_gain, conv_shift, w_proj, out_gain, out_shift):
    rows, width = stream.shape[0], w_value.shape[1]
    gathers = 2 * LAYERS
    bf16, f32 = jnp.bfloat16, jnp.float32
    dma = pltpu.SemaphoreType.DMA
    return pl.pallas_call(
        functools.partial(kernel, ns),
        out_shape=jax.ShapeDtypeStruct((rows, LANES), bf16),
        in_specs=[pl.BlockSpec(memory_space=pl.ANY)] * 10,
        out_specs=pl.BlockSpec(memory_space=pltpu.VMEM),
        scratch_shapes=[
            pltpu.VMEM((gathers, PEERS, rows, LANES), bf16),
            pltpu.VMEM((LAYERS, width, 2 * LANES), bf16),
            pltpu.VMEM((LAYERS, width, LANES), bf16),
            pltpu.VMEM((LAYERS, KERNEL, LANES), bf16),
            pltpu.VMEM((LAYERS, width), f32),
            pltpu.VMEM((LAYERS, width), f32),
            pltpu.VMEM((LAYERS, width), f32),
            pltpu.VMEM((LAYERS, width), f32),
            pltpu.VMEM((1, rows), jnp.int32),
            pltpu.VMEM((rows + 2 * PAD, LANES), f32),
            pltpu.VMEM((rows, LANES), f32),
            pltpu.VMEM((rows, LANES), f32),
            pltpu.VMEM((LAYERS, rows + 2 * PAD, LANES), f32),
            pltpu.VMEM((LAYERS, 2, PAD, LANES), bf16),
            pltpu.VMEM((LAYERS, 2, PAD, LANES), bf16),
            pltpu.VMEM((PEERS, rows, LANES), bf16),
            pltpu.VMEM((rows, LANES), f32),
            pltpu.VMEM((rows, LANES), f32),
            pltpu.VMEM((2, rows), f32),
            pltpu.VMEM((2, rows), f32),
            pltpu.VMEM((PEERS, 2, rows), f32),
            dma((7 + 3 * LAYERS,)),
            dma((gathers, 2 * CHUNKS)),
            dma((gathers, 2 * CHUNKS, SIDE)),
            dma((LAYERS, 2)),
            dma((LAYERS, 2)),
            dma((2,)),
            dma((2,)),
            dma((PEERS,)),
            dma((PEERS,)),
        ],
        compiler_params=pltpu.CompilerParams(
            collective_id=0, has_side_effects=True, vmem_limit_bytes=60 * 1024 * 1024
        ),
        name="stack",
    )(stream, doc_ids.reshape(1, rows), w_value, w_gate, conv_kernel, conv_gain, conv_shift, w_proj, out_gain, out_shift)


def solution(mesh):
    return jax.shard_map(
        functools.partial(on_device, mesh.shape["sp"]),
        mesh=mesh,
        in_specs=(
            P("sp", "tp"), P("sp"), P(None, None, "tp"), P(None, None, "tp"), P(None, None, "tp"), P(), P(),
            P(None, None, "tp"), P(), P(),
        ),
        out_specs=P("sp", "tp"),
        check_vma=False,
    )
```

time: 133 us -> 98.9 us (0.74)
  Pallas kernels: 130 us -> 96 us
    pallas_call x1, Pallas kernels: 130 us -> 96 us  [on_device(): pl.pallas_call(functools.partial(kernel, ns), out_shape=jax.ShapeDtypeStr...]
where the time goes in v2:
time: 98.9 us; the launch traced here: 98.8 us
  Pallas kernels  96 us (97%)
  local copies, waits for them, and re-layouts  2.78 us (3%)
    pallas_call x1, Pallas kernels, on_device(): pl.pallas_call(functools.partial(kernel, ns), out_shape=jax.ShapeDtypeStr...  96 us

profile of v2, /device:TPU:2, one launch (start us, length us, event | category | flops | bytes accessed | tf_op | source)
XLA Modules:
  0.0 98.8 jit_solution(17701624649018547258)
XLA Ops:
  0.0 1.2 %reshape.3.doc = s32[1,384]{1,0:T(1,128)} reshape(s32[384]{0:T(512)} %param.11) | data formatting | bytes 3072 | tf_op jit(solution)/shard_map/reshape | solution.py:433
  1.2 96.0 %stack.1 = bf16[384,128]{1,0:T(8,128)(2,1)} custom-call(bf16[384,128]{1,0:T(8,128)(2,1)} %stream.1, s32[1,384]{1,0:T(1,128)} %reshape.3.doc, bf16[3,2048,128]{2,1,0:T(8,128)(2,1)} %wv.1, bf16[3,2048,128]{2,1,0:T(8,128)(2,1)} %wg.1, bf16[3,31,128]{2,1,0:T(8,128)(2,1)} %ck.1, f32[3,2048]{1,0:T(4,128)} %cg.1, f32[3,2048]{1,0:T(4,128)} %cs.1, ...), custom_call_target="tpu_custom_call" | custom-call | tf_op jit(solution)/shard_map/stack/pallas_call | solution.py:392
  97.2 1.5 %copy.12 = bf16[384,128]{1,0:T(8,128)(2,1)} copy(bf16[384,128]{1,0:T(8,128)(2,1)} %stack.1) | data formatting | bytes 196608

commit v3 on v2

--- a/solution.py
+++ b/solution.py
@@ -15,17 +15,21 @@
 SIDE = 4
 PEERS = SIDE * SIDE
 STEPS = (1, -1, 2)
-CHUNKS = 3
+SENDS = (2, 1, -1)
+FAR_FIRST = [(du, dv) for du in (2, 1, -1, 0) for dv in (2, 1, -1, 0) if (du, dv) != (0, 0)]
+CHUNKS = 4
 OUTER = 80
 MIDDLE = 144
+STAGGER = False
+DIRECT = (True, False, False, False)
 ALPHA = 2.0**0.25
 EPS = 1e-05
 MESH = pl.DeviceIdType.MESH
 
 
 class Spread:
-    def __init__(self, env, stage, piece, row0, rows, x_first):
-        self.env, self.k, self.p = env, stage, piece
+    def __init__(self, env, stage, piece, row0, rows, x_first, direct):
+        self.env, self.k, self.p, self.direct = env, stage, piece, direct
         self.row0, self.rows, self.x_first = row0, rows, x_first
 
     def at(self, du, dv):
@@ -49,23 +53,26 @@
 
     def spread(self, du):
         mine = self.ref(self.at(du, 0))
-        for dv in (2, 1, -1):
+        for dv in SENDS:
             self.copy(mine, mine, 3, self.at(0, dv)).start()
 
     def start(self):
         mine = self.ref(self.at(0, 0))
-        for n, du in enumerate(STEPS):
-            self.copy(mine, mine, n, self.at(-du, 0)).start()
+        if self.direct:
+            for du, dv in FAR_FIRST:
+                self.copy(mine, mine, 3, self.at(du, dv)).start()
+            return
+        for du in SENDS:
+            self.copy(mine, mine, STEPS.index(du), self.at(-du, 0)).start()
         self.spread(0)
 
-    def turn(self):
-        for n, du in enumerate(STEPS):
-            block = self.ref(self.at(du, 0))
-            self.copy(block, block, n, self.at(1, 0)).wait_recv()
-            self.spread(du)
+    def turn(self, du):
+        block = self.ref(self.at(du, 0))
+        self.copy(block, block, STEPS.index(du), self.at(1, 0)).wait_recv()
+        self.spread(du)
 
     def finish(self):
-        many = self.ref(pl.ds(0, PEERS - SIDE))
+        many = self.ref(pl.ds(0, PEERS - 1 if self.direct else PEERS - SIDE))
         self.copy(many, many, 3, self.at(1, 0)).wait_recv()
 
     def drain(self):
@@ -78,42 +85,30 @@
     cuts = []
     for k in range(2 * LAYERS):
         lost = PAD * ((k + 1) // 2)
-        cuts.append((0, outer - lost, middle - lost, rows // 2))
+        cuts.append((0, PAD, outer - lost, middle - lost, rows // 2))
     return cuts
 
 
-def plan(cuts):
-    now, link, order = 0.0, 0.0, []
-    ready = {("turn", c, 0): 3.0 + 0.5 * c for c in range(CHUNKS)}
-    done = set()
-
-    def rows_of(c, k):
-        return 2 * (cuts[k][c + 1] - cuts[k][c])
-
-    while ready:
-        allowed = [
-            step for step in ready
-            if step[0] != "conv" or all(("finish", c, step[2]) in done for c in range(step[1]))
-        ]
-        step = min(allowed, key=lambda each: (max(ready[each], now), ready[each], each[1]))
-        what, c, k = step
-        now = max(now, ready.pop(step))
-        order.append(step)
-        done.add(step)
-        if what == "turn":
-            now += 0.15
-            link = max(now + 3.0, link) + 0.02 * rows_of(c, k)
-            ready["finish", c, k] = link
-        elif what == "finish" and k % 2 == 0:
-            now += 0.4 + 0.005 * rows_of(c, k)
-            ready["conv", c, k] = now + (2.5 if c == 0 else 0.0)
-        elif what == "finish":
-            now += 0.4 + 0.008 * rows_of(c, k)
-            if k + 1 < 2 * LAYERS:
-                ready["turn", c, k + 1] = now + 3.0
-        else:
-            now += 0.2 + 0.003 * rows_of(c, k)
-            ready["turn", c, k + 1] = now + 3.0
+def plan():
+    order = [("turn", 1, 0), ("turn", 2, 0), ("finish", 0, 0), ("turn", 3, 0)]
+    last = 2 * LAYERS - 1
+    for k in range(last + 1):
+        conv = k % 2 == 0
+        order.append(("finish", 1, k))
+        if conv:
+            order += [("conv", 1, k), ("conv", 0, k)]
+        order.append(("finish", 2, k))
+        if conv:
+            order.append(("conv", 2, k))
+        if STAGGER and k < last:
+            order += [("turn", 1, k + 1), ("finish", 0, k + 1)]
+        order.append(("finish", 3, k))
+        if conv:
+            order.append(("conv", 3, k))
+        if k < last:
+            if not STAGGER:
+                order += [("turn", 1, k + 1), ("finish", 0, k + 1)]
+            order += [("turn", 2, k + 1), ("turn", 3, k + 1)]
     return order
 
 
@@ -167,8 +162,8 @@
         for c in range(CHUNKS):
             low, high = cuts[k][c], cuts[k][c + 1]
             pieces[c, k] = (
-                Spread(env, k, 2 * c, low, high - low, True),
-                Spread(env, k, 2 * c + 1, rows - high, high - low, False),
+                Spread(env, k, 2 * c, low, high - low, True, DIRECT[c]),
+                Spread(env, k, 2 * c + 1, rows - high, high - low, False, DIRECT[c]),
             )
 
     def start(c, k):
@@ -186,41 +181,39 @@
     loads[1].wait()
     for n in range(rows // LANES):
         docs[PAD + n * LANES : PAD + (n + 1) * LANES, :] = column(
-            docv[0:1, n * LANES : (n + 1) * LANES].astype(jnp.float32)
+            docv[n * LANES : (n + 1) * LANES].astype(jnp.float32).reshape(1, LANES)
         )
     right_doc = halo(docs.at[pl.ds(rows, PAD)], docs.at[pl.ds(0, PAD)], dss.at[0], drs.at[0], after)
     left_doc = halo(docs.at[pl.ds(PAD, PAD)], docs.at[pl.ds(rows + PAD, PAD)], dss.at[1], drs.at[1], before)
     right_doc.start()
     left_doc.start()
-    for c in loads[2:]:
-        c.wait()
-    for group in weights:
-        for c in group:
+    def prepare():
+        for c in loads[2:]:
             c.wait()
-    right_doc.wait()
-    left_doc.wait()
-
-    @pl.when(s == 0)
-    def _():
-        docs[0:PAD, :] = jnp.full((PAD, LANES), -1.0, jnp.float32)
-
-    @pl.when(s == ns - 1)
-    def _():
-        docs[rows + PAD : rows + 2 * PAD, :] = jnp.full((PAD, LANES), -1.0, jnp.float32)
-
-    def reach(n, carry):
-        base = pl.multiple_of(n * PAD, PAD)
-        mine = docs[pl.ds(base + PAD, PAD), :]
-        low = jnp.zeros((PAD, LANES), jnp.float32)
-        high = jnp.zeros((PAD, LANES), jnp.float32)
-        for j in range(1, HALF + 1):
-            low = low + (docs[pl.ds(base + PAD - j, PAD), :] == mine).astype(jnp.float32)
-            high = high + (docs[pl.ds(base + PAD + j, PAD), :] == mine).astype(jnp.float32)
-        nleft[pl.ds(base, PAD), :] = low
-        nright[pl.ds(base, PAD), :] = high
-        return carry
-
-    lax.fori_loop(0, rows // PAD, reach, 0)
+        right_doc.wait()
+        left_doc.wait()
+
+        @pl.when(s == 0)
+        def _():
+            docs[0:PAD, :] = jnp.full((PAD, LANES), -1.0, jnp.float32)
+
+        @pl.when(s == ns - 1)
+        def _():
+            docs[rows + PAD : rows + 2 * PAD, :] = jnp.full((PAD, LANES), -1.0, jnp.float32)
+
+        def reach(n, carry):
+            base = pl.multiple_of(n * PAD, PAD)
+            mine = docs[pl.ds(base + PAD, PAD), :]
+            low = jnp.zeros((PAD, LANES), jnp.float32)
+            high = jnp.zeros((PAD, LANES), jnp.float32)
+            for j in range(1, HALF + 1):
+                low = low + (docs[pl.ds(base + PAD - j, PAD), :] == mine).astype(jnp.float32)
+                high = high + (docs[pl.ds(base + PAD + j, PAD), :] == mine).astype(jnp.float32)
+            nleft[pl.ds(base, PAD), :] = low
+            nright[pl.ds(base, PAD), :] = high
+            return carry
+
+        lax.fori_loop(0, rows // PAD, reach, 0)
 
     def conv_rows(layer, first, last):
         def tile(n, carry):
@@ -251,12 +244,16 @@
         mean = jnp.sum(one, axis=1, keepdims=True) * (1.0 / width)
         var = jnp.maximum(jnp.sum(two, axis=1, keepdims=True) * (1.0 / width) - mean * mean, 0.0)
         scale = lax.rsqrt(var + EPS)
+        centre = mean * scale
         for j in range(PEERS):
             v = gbuf[k, j, part, :].astype(jnp.float32)
             cols = slice(j * LANES, (j + 1) * LANES)
-            v = (v - mean) * scale * gain[layer : layer + 1, cols] + shift[layer : layer + 1, cols]
+            factor, offset = gain[layer : layer + 1, cols], shift[layer : layer + 1, cols]
             if silu:
-                v = v / (1.0 + jnp.exp(-v))
+                factor, offset = 0.5 * factor, 0.5 * offset
+            v = (v * scale - centre) * factor + offset
+            if silu:
+                v = v + v * jnp.tanh(v)
             act[j, part, :] = v.astype(jnp.bfloat16)
 
     def halos(layer):
@@ -272,8 +269,17 @@
         rows_of = [jnp.concatenate([ref[j, part, :] for j in range(PEERS)], axis=1) for part in parts]
         return jnp.concatenate(rows_of, axis=0)
 
+    pending = {(layer, n) for layer in range(LAYERS) for n in range(2)}
+
+    def loaded(layer, n):
+        if (layer, n) in pending:
+            pending.remove((layer, n))
+            for c in weights[layer][2:] if n else weights[layer][:2]:
+                c.wait()
+
     def gated(c, k):
         layer, parts = k // 2, sides(c, k)
+        loaded(layer, 0)
         if layer == 0:
             lhs = joined(gbuf.at[0], parts)
             for part in parts:
@@ -299,8 +305,6 @@
         layer = k // 2
         left, right = sides(c, k + 1)
         if c == 0:
-            conv_rows(layer, left.start + PAD, left.stop)
-            conv_rows(layer, right.start, right.stop - PAD)
             for h in halos(layer):
                 h.wait()
             glu[layer, 0:PAD, :] = hrecv[layer, 0].astype(jnp.float32)
@@ -315,6 +319,7 @@
 
     def projected(c, k):
         layer, parts = k // 2, sides(c, k)
+        loaded(layer, 1)
         for part in parts:
             normed(k, layer, cgv, csv, True, part)
         branch = jnp.dot(joined(act, parts), wpb[layer], preferred_element_type=jnp.float32)
@@ -326,10 +331,18 @@
             else:
                 z32[part, :] = z
 
-    for what, c, k in plan(cuts):
+    order = plan()
+    waiting = CHUNKS - sum(DIRECT)
+    for what, c, k in order:
+        if waiting and what == "turn":
+            waiting -= 1
+        elif waiting == 0 or (waiting and what == "conv"):
+            prepare()
+            waiting = None
         if what == "turn":
-            for piece in pieces[c, k]:
-                piece.turn()
+            for du in STEPS:
+                for piece in pieces[c, k]:
+                    piece.turn(du)
         elif what == "finish":
             for piece in pieces[c, k]:
                 piece.finish()
@@ -403,7 +416,7 @@
             pltpu.VMEM((LAYERS, width), f32),
             pltpu.VMEM((LAYERS, width), f32),
             pltpu.VMEM((LAYERS, width), f32),
-            pltpu.VMEM((1, rows), jnp.int32),
+            pltpu.VMEM((rows,), jnp.int32),
             pltpu.VMEM((rows + 2 * PAD, LANES), f32),
             pltpu.VMEM((rows, LANES), f32),
             pltpu.VMEM((rows, LANES), f32),
@@ -430,7 +443,7 @@
             collective_id=0, has_side_effects=True, vmem_limit_bytes=60 * 1024 * 1024
         ),
         name="stack",
-    )(stream, doc_ids.reshape(1, rows), w_value, w_gate, conv_kernel, conv_gain, conv_shift, w_proj, out_gain, out_shift)
+    )(stream, doc_ids, w_value, w_gate, conv_kernel, conv_gain, conv_shift, w_proj, out_gain, out_shift)
 
 
 def solution(mesh):

time: 98.9 us -> 91 us (0.920)
  Pallas kernels: 96 us -> 89.3 us
  local copies, waits for them, and re-layouts: 2.78 us -> 1.54 us
    pallas_call x1, Pallas kernels: 96 us -> 89.3 us  [on_device(): pl.pallas_call(functools.partial(kernel, ns), out_shape=jax.ShapeDtypeStr...]
    reshape x1 -> x0, local copies, waits for them, and re-layouts: 1.24 us -> none  [on_device(): doc_ids.reshape(1, rows)]
where the time goes in v3:
time: 91 us; the launch traced here: 90.8 us
  Pallas kernels  89.3 us (98%)
  local copies, waits for them, and re-layouts  1.54 us (2%)
    pallas_call x1, Pallas kernels, on_device(): pl.pallas_call(functools.partial(kernel, ns), out_shape=jax.ShapeDtypeStr...  89.3 us

profile of v3, /device:TPU:2, one launch (start us, length us, event | category | flops | bytes accessed | tf_op | source)
XLA Modules:
  0.0 90.8 jit_solution(12311002894596972090)
XLA Ops:
  0.0 89.3 %stack.1 = bf16[384,128]{1,0:T(8,128)(2,1)} custom-call(bf16[384,128]{1,0:T(8,128)(2,1)} %stream.1, s32[384]{0:T(512)} %doc.1, bf16[3,2048,128]{2,1,0:T(8,128)(2,1)} %wv.1, bf16[3,2048,128]{2,1,0:T(8,128)(2,1)} %wg.1, bf16[3,31,128]{2,1,0:T(8,128)(2,1)} %ck.1, f32[3,2048]{1,0:T(4,128)} %cg.1, f32[3,2048]{1,0:T(4,128)} %cs.1, bf16[3,2048,128]{2,1,0:T(8,128)(2,1)} %wp.1, ...), custom_call_target="tpu_custom_call" | custom-call | tf_op jit(solution)/shard_map/stack/pallas_call | solution.py:405
  89.3 1.5 %copy.12 = bf16[384,128]{1,0:T(8,128)(2,1)} copy(bf16[384,128]{1,0:T(8,128)(2,1)} %stack.1) | data formatting | bytes 196608

commit v4 on v3

--- a/solution.py
+++ b/solution.py
@@ -18,9 +18,9 @@
 SENDS = (2, 1, -1)
 FAR_FIRST = [(du, dv) for du in (2, 1, -1, 0) for dv in (2, 1, -1, 0) if (du, dv) != (0, 0)]
 CHUNKS = 4
-OUTER = 80
-MIDDLE = 144
-STAGGER = False
+OUTER = 96
+MIDDLE = 160
+EDGE_AFTER = 1
 DIRECT = (True, False, False, False)
 ALPHA = 2.0**0.25
 EPS = 1e-05
@@ -90,25 +90,20 @@
 
 
 def plan():
-    order = [("turn", 1, 0), ("turn", 2, 0), ("finish", 0, 0), ("turn", 3, 0)]
+    inner = range(1, CHUNKS)
+    order = [("turn", c, 0) for c in inner]
+    order.insert(2, ("finish", 0, 0))
     last = 2 * LAYERS - 1
     for k in range(last + 1):
-        conv = k % 2 == 0
-        order.append(("finish", 1, k))
-        if conv:
-            order += [("conv", 1, k), ("conv", 0, k)]
-        order.append(("finish", 2, k))
-        if conv:
-            order.append(("conv", 2, k))
-        if STAGGER and k < last:
+        for c in inner:
+            order.append(("finish", c, k))
+            if k % 2 == 0:
+                order.append(("conv", c, k))
+                if c == EDGE_AFTER:
+                    order.append(("conv", 0, k))
+        if k < last:
             order += [("turn", 1, k + 1), ("finish", 0, k + 1)]
-        order.append(("finish", 3, k))
-        if conv:
-            order.append(("conv", 3, k))
-        if k < last:
-            if not STAGGER:
-                order += [("turn", 1, k + 1), ("finish", 0, k + 1)]
-            order += [("turn", 2, k + 1), ("turn", 3, k + 1)]
+            order += [("turn", c, k + 1) for c in inner[1:]]
     return order
 
 

time: 91 us -> 90.1 us (level)
  the two profiles are of different devices: /device:TPU:2 before, /device:TPU:8 now
where the time goes in v4:
time: 90.1 us; the launch traced here: 90 us
  Pallas kernels  88.4 us (98%)
  local copies, waits for them, and re-layouts  1.54 us (2%)
    pallas_call x1, Pallas kernels, on_device(): pl.pallas_call(functools.partial(kernel, ns), out_shape=jax.ShapeDtypeStr...  88.4 us

profile of v4, /device:TPU:8, one launch (start us, length us, event | category | flops | bytes accessed | tf_op | source)
XLA Modules:
  0.0 90.0 jit_solution(6002073270537604393)
XLA Ops:
  0.0 88.4 %stack.1 = bf16[384,128]{1,0:T(8,128)(2,1)} custom-call(bf16[384,128]{1,0:T(8,128)(2,1)} %stream.1, s32[384]{0:T(512)} %doc.1, bf16[3,2048,128]{2,1,0:T(8,128)(2,1)} %wv.1, bf16[3,2048,128]{2,1,0:T(8,128)(2,1)} %wg.1, bf16[3,31,128]{2,1,0:T(8,128)(2,1)} %ck.1, f32[3,2048]{1,0:T(4,128)} %cg.1, f32[3,2048]{1,0:T(4,128)} %cs.1, bf16[3,2048,128]{2,1,0:T(8,128)(2,1)} %wp.1, ...), custom_call_target="tpu_custom_call" | custom-call | tf_op jit(solution)/shard_map/stack/pallas_call | solution.py:400
  88.4 1.5 %copy.12 = bf16[384,128]{1,0:T(8,128)(2,1)} copy(bf16[384,128]{1,0:T(8,128)(2,1)} %stack.1) | data formatting | bytes 196608

commit v5 on v4

--- a/solution.py
+++ b/solution.py
@@ -285,7 +285,8 @@
                 keep[part, :] = act[t, part, :].astype(jnp.float32)
             lhs = joined(act, parts)
         both = jnp.dot(lhs, wvg[layer], preferred_element_type=jnp.float32)
-        value = (both[:, :LANES] / (1.0 + jnp.exp(-both[:, LANES:]))).astype(jnp.bfloat16)
+        half_lin = 0.5 * both[:, :LANES]
+        value = (half_lin + half_lin * jnp.tanh(0.5 * both[:, LANES:])).astype(jnp.bfloat16)
         count = pieces[c, k][0].rows
         for n, part in enumerate(parts):
             mine = value[n * count : (n + 1) * count]
@@ -359,7 +360,8 @@
     stsend[0:1, :] = one[0:1, :]
     stsend[1:2, :] = two[0:1, :]
     outgoing = []
-    for d in range(1, PEERS):
+    peers = sorted(range(1, PEERS), key=lambda d: abs(d - PEERS // 2 - 2))
+    for d in peers:
         c = pltpu.make_async_remote_copy(
             src_ref=stsend,
             dst_ref=strecv.at[d],
@@ -371,8 +373,8 @@
         c.start()
         outgoing.append(c)
     sums = stsend[...]
-    for d in range(1, PEERS):
-        outgoing[d - 1].wait_recv()
+    for n, d in enumerate(peers):
+        outgoing[n].wait_recv()
         sums = sums + strecv[d]
     stat[...] = sums
     mine = pl.ds(pl.multiple_of(t * LANES, LANES), LANES)

time: 90.1 us -> 90.3 us (level)
  the two profiles are of different devices: /device:TPU:8 before, /device:TPU:2 now
where the time goes in v5:
time: 90.3 us; the launch traced here: 90.2 us
  Pallas kernels  88.6 us (98%)
  local copies, waits for them, and re-layouts  1.54 us (2%)
    pallas_call x1, Pallas kernels, on_device(): pl.pallas_call(functools.partial(kernel, ns), out_shape=jax.ShapeDtypeStr...  88.6 us

profile of v5, /device:TPU:2, one launch (start us, length us, event | category | flops | bytes accessed | tf_op | source)
XLA Modules:
  0.0 90.2 jit_solution(13425595330295029548)
XLA Ops:
  0.0 88.6 %stack.1 = bf16[384,128]{1,0:T(8,128)(2,1)} custom-call(bf16[384,128]{1,0:T(8,128)(2,1)} %stream.1, s32[384]{0:T(512)} %doc.1, bf16[3,2048,128]{2,1,0:T(8,128)(2,1)} %wv.1, bf16[3,2048,128]{2,1,0:T(8,128)(2,1)} %wg.1, bf16[3,31,128]{2,1,0:T(8,128)(2,1)} %ck.1, f32[3,2048]{1,0:T(4,128)} %cg.1, f32[3,2048]{1,0:T(4,128)} %cs.1, bf16[3,2048,128]{2,1,0:T(8,128)(2,1)} %wp.1, ...), custom_call_target="tpu_custom_call" | custom-call | tf_op jit(solution)/shard_map/stack/pallas_call | solution.py:402
  88.6 1.5 %copy.12 = bf16[384,128]{1,0:T(8,128)(2,1)} copy(bf16[384,128]{1,0:T(8,128)(2,1)} %stack.1) | data formatting | bytes 196608
